TPU v7x, 32 devices: a whole 2x2x4 slice. The times are simulated.
32 devices in a mesh: sp: 8 (over z, x), tp: 4 (over y, core).
Axes of the slice: x: 2, y: 2, z: 4, core: 2. Of those that a mesh axis runs over, the one named last changes fastest.
Arguments:
- stream: bfloat16 [4096, 2048], P(('sp', 'tp')), may hold values from -6 to 6
- pool_in: bfloat16 [4096, 1024], P('sp', 'tp'), may hold values from -6 to 6
- doc_ids: int32 [4096], P('sp'), may hold values from 0 to 7, never falling along the last dimension, each value on 1 to 1024 neighbouring positions
- pool_map: bfloat16 [4, 256, 512], P('tp'), may hold values from -0.375 to 0.375
- pool_scale: float32 [2048], P('tp'), may hold values from 0.1 to 1.9
- out_weight: bfloat16 [2048, 2048], P('tp'), may hold values from -0.125 to 0.125
- norm_gain: float32 [2048], replicated, may hold values from 0.1 to 1.9
- routes: int32 [4096, 2], P('sp'), may hold values from 0 to 7, all different within a row; in each aligned block of 128 rows (0 to 127, 128 to 255, ...) at most 48 rows name the same one
- route_weight: float32 [4096, 2], P(('sp', 'tp')), may hold values from 0.2 to 1
- expert_gate: bfloat16 [8, 2048, 1024], P('sp', None, 'tp'), may hold values from -0.125 to 0.125
- expert_up: bfloat16 [8, 2048, 1024], P('sp', None, 'tp'), may hold values from -0.125 to 0.125
- expert_down: bfloat16 [8, 1024, 2048], P('sp', 'tp'), may hold values from -0.1875 to 0.1875
Outputs:
- result: bfloat16 [4096, 2048], P(('sp', 'tp'))
Inputs may be any that keep to these rules, and one draw needn't show every extreme that they name: `routes`: each token names 2 different experts; in each aligned block of 128 rows no expert is named by more than 48 rows, a bound that some block reaches. `doc_ids`: never falling; each document holds at most 1024 positions.
All inputs are finite; a program needn't handle non-finite values.
Results may differ from a plain program's by a relative error of at most 0.014.
Values may be sent and summed in bfloat16 or wider, within the bound.
A program may use at most 64 MiB of HBM per device.

v0:
```python
import jax
import jax.numpy as jnp
from jax import lax
from jax.sharding import PartitionSpec as P

SPAN = 16


EPS = 1e-06


def passed_along(value, axis, by):
    length = lax.axis_size(axis)
    pairs = [(i, i + by) for i in range(length) if 0 <= i + by < length]
    return lax.ppermute(value, axis, pairs)


def slot_table(route_block, expert_count, capacity, top_count):
    flattened = route_block.reshape(-1)
    one_hot = (flattened[:, None] == jnp.arange(expert_count, dtype=jnp.int32)[None, :]).astype(
        jnp.int32
    )
    ranking = jnp.sum((jnp.cumsum(one_hot, axis=0) - one_hot) * one_hot, axis=1)
    target_slot = flattened * capacity + ranking
    matches = target_slot[None, :] == jnp.arange(expert_count * capacity, dtype=jnp.int32)[:, None]
    sources = jnp.sum(
        jnp.where(matches, jnp.arange(flattened.shape[0], dtype=jnp.int32)[None, :], 0), axis=1
    )
    filled = jnp.any(matches, axis=1)
    return (target_slot, sources // top_count, filled)


def per_device(
    stream,
    pool_in,
    doc_ids,
    pool_map,
    pool_scale,
    out_weight,
    norm_gain,
    routes,
    route_weight,
    expert_gate,
    expert_up,
    expert_down,
):
    row_count = pool_in.shape[0]
    model_width = stream.shape[1]
    top_count = routes.shape[1]
    tp_count = lax.axis_size("tp")
    expert_count = lax.axis_size("sp")
    quarter = row_count // tp_count
    capacity = max(2, 3 * top_count * quarter // (2 * expert_count))
    reach_rows = SPAN - 1
    tail_rows = (
        pool_in[row_count - reach_rows :],
        doc_ids[row_count - reach_rows :].astype(jnp.bfloat16),
    )
    prior_rows, prior_docs = passed_along((tail_rows[0], tail_rows[1]), "sp", 1)
    extended = jnp.concatenate([prior_rows, pool_in], axis=0).astype(jnp.float32)
    extended_docs = jnp.concatenate([prior_docs.astype(jnp.float32), doc_ids.astype(jnp.float32)])
    own_docs = doc_ids.astype(jnp.float32)
    window = jnp.left_shift(jnp.int32(2), lax.axis_index("tp"))
    positions = lax.axis_index("sp") * row_count + jnp.arange(row_count, dtype=jnp.int32)
    running = jnp.zeros(pool_in.shape, jnp.float32)
    counts = jnp.zeros((row_count,), jnp.float32)
    for offset in range(reach_rows + 1):
        begin_row = reach_rows - offset
        piece_rows = extended[begin_row : begin_row + row_count]
        piece_docs = extended_docs[begin_row : begin_row + row_count]
        in_window = (offset < window) & (positions - offset >= 0) & (piece_docs == own_docs)
        running = running + jnp.where(in_window[:, None], piece_rows, 0.0)
        counts = counts + in_window.astype(jnp.float32)
    pooled = (running / counts[:, None] - pool_in.astype(jnp.float32)).astype(jnp.bfloat16)
    branch = (jnp.dot(pooled, pool_map[0], preferred_element_type=jnp.float32) * pool_scale).astype(
        jnp.bfloat16
    )
    projected = lax.psum_scatter(
        jnp.dot(branch, out_weight, preferred_element_type=jnp.float32).astype(jnp.bfloat16),
        "tp",
        scatter_dimension=0,
        tiled=True,
    ).astype(jnp.float32)
    mixed_rows = (stream.astype(jnp.float32) + projected).astype(jnp.bfloat16)
    mixed_up = mixed_rows.astype(jnp.float32)
    normed = (
        mixed_up * lax.rsqrt(jnp.mean(mixed_up * mixed_up, axis=1, keepdims=True) + EPS) * norm_gain
    ).astype(jnp.bfloat16)
    own_routes = lax.dynamic_slice_in_dim(routes, lax.axis_index("tp") * quarter, quarter, 0)
    own_slots, own_sources, own_filled = slot_table(own_routes, expert_count, capacity, top_count)
    token_index = own_sources.reshape(expert_count, 1, capacity)
    filled_slots = own_filled.reshape(expert_count, 1, capacity)
    dispatch = jnp.where(filled_slots[..., None], normed[token_index], jnp.zeros((), jnp.bfloat16))
    arrived = lax.all_to_all(dispatch, "sp", split_axis=0, concat_axis=0, tiled=True)
    arrived = lax.all_gather(arrived, "tp", axis=1, tiled=True)
    stacked = arrived.reshape(-1, model_width)
    gate_pre = jnp.dot(stacked, expert_gate[0], preferred_element_type=jnp.float32)
    up_pre = jnp.dot(stacked, expert_up[0], preferred_element_type=jnp.float32)
    hidden = (jax.nn.silu(gate_pre) * up_pre).astype(jnp.bfloat16)
    partial_out = jnp.dot(hidden, expert_down[0], preferred_element_type=jnp.float32).reshape(
        arrived.shape
    )
    summed = lax.psum_scatter(
        partial_out.astype(jnp.bfloat16), "tp", scatter_dimension=1, tiled=True
    )
    returned = lax.all_to_all(summed, "sp", split_axis=0, concat_axis=0, tiled=True)
    outputs = returned.reshape(expert_count * capacity, model_width)
    picked = outputs[own_slots].astype(jnp.float32).reshape(quarter, top_count, model_width)
    combined = jnp.sum(route_weight[:, :, None] * picked, axis=1)
    return (mixed_up + combined).astype(jnp.bfloat16)


def solution(mesh):
    in_specs = (
        P(("sp", "tp"), None),
        P("sp", "tp"),
        P("sp"),
        P("tp", None, None),
        P("tp"),
        P("tp", None),
        P(),
        P("sp", None),
        P(("sp", "tp"), None),
        P("sp", None, "tp"),
        P("sp", None, "tp"),
        P("sp", "tp", None),
    )
    out_specs = P(("sp", "tp"), None)
    return jax.shard_map(
        per_device, mesh=mesh, in_specs=in_specs, out_specs=out_specs, check_vma=False
    )
```

profile of v0, /device:TPU:11, one launch (start us, length us, event | category | flops | bytes accessed | tf_op | source)
XLA Modules:
  0.0 345.5 jit_solution(15790162782947919456)
XLA Ops:
  6.5 0.8 fusion.126
  7.5 3.2 collective-permute-start.1
  10.6 0.7 slice.106
  11.3 3.1 collective-permute-start
  14.6 0.8 convert_add_fusion.1
  15.4 0.3 collective-permute-done
  15.7 1.0 maximum_convert_fusion
  16.7 5.4 %convolution_convert_fusion.1 = bf16[512,2048]{1,0:T(8,128)(2,1)} fusion(bf16[512,2048]{1,0:T(8,128)(2,1)S(1)} %copy-done, f32[512]{0:T(512)} %param.16, bf16[512,256]{1,0:T(8,128)(2,1)} %param.13, f32[527,256]{1,0:T(8,128)S(1)} %maximum_convert_fusion, bf16[1,256,512]{2,1,0:T(8,128)(2,1)} %param.15, f32[512]{0:T(512)S(1)} %get-tuple-element.7, ...), kind=kOutput, calls=%fused_computation.3 | convolution fusion | flops 1214119936 | bytes 13119488 | tf_op jit(solution)/shard_map/dot_general | solution.py:79
  22.2 0.7 broadcast_multiply_fusion
  23.4 0.6 reduce-window.6
  24.0 0.2 slice_reduce_fusion
  24.7 0.2 fusion.29
  24.9 30.9 %reduce-scatter.5.cloned.1.call-done = bf16[128,2048]{1,0:T(8,128)(2,1)} async-done(((bf16[512,2048]{1,0:T(8,128)(2,1)}), bf16[128,2048]{1,0:T(8,128)(2,1)}) %reduce-scatter.5.cloned.1.call-update) | async-done | bytes 524304 | tf_op jit(solution)/shard_map/reduce_scatter | solution.py:78
  55.8 1.3 fusion.2
  57.1 1.3 fusion.4
  58.4 3.1 gather_fusion
  61.5 1.6 broadcast_select_fusion
  63.1 39.2 %all_to_all.10 = bf16[8,1,48,2048]{3,2,1,0:T(8,128)(2,1)} all-to-all(bf16[8,1,48,2048]{3,2,1,0:T(8,128)(2,1)S(1)} %broadcast_select_fusion), channel_id=1, replica_groups=mesh['sp'=8,'tp'=4] {'sp'}, dimensions={0} | all-to-all | bytes 3145728 | tf_op jit(solution)/shard_map/all_to_all | solution.py:94
  102.4 48.2 %all-gather.2.cloned.1.call-done = bf16[8,4,48,2048]{3,2,1,0:T(8,128)(2,1)} async-done(((bf16[8,1,48,2048]{3,2,1,0:T(8,128)(2,1)}), bf16[8,4,48,2048]{3,2,1,0:T(8,128)(2,1)}) %all-gather.2.cloned.1.call-update) | async-done | bytes 6291472 | tf_op jit(solution)/shard_map/all_gather | solution.py:95
  150.6 5.0 %fusion.8 = f32[1536,256]{1,0:T(8,128)S(1)} fusion(bf16[1536,2048]{1,0:T(8,128)(2,1)} %bitcast.52, bf16[1,2048,256]{2,1,0:T(8,128)(2,1)} %param.21), kind=kOutput, calls=%fused_computation.19 | convolution fusion | flops 1610612736 | bytes 8912896 | tf_op jit(solution)/shard_map/dot_general | solution.py:97
  155.8 2.1 fusion
  157.9 4.5 %convolution_convert_fusion = bf16[8,4,48,2048]{3,2,1,0:T(8,128)(2,1)} fusion(bf16[8,4,48,256]{3,2,1,0:T(8,128)(2,1)S(1)} %bitcast.49, bf16[1,256,2048]{2,1,0:T(8,128)(2,1)S(1)} %copy-done.3), kind=kOutput, calls=%fused_computation.2 | convolution fusion | flops 1613758464 | bytes 8126464 | tf_op jit(solution)/shard_map/dot_general | solution.py:100
  162.4 0.6 copy-done.8
  163.0 0.6 dynamic-slice
  163.6 117.7 %all-reduce.3.cloned.1.call-done = bf16[8,4,48,2048]{3,2,1,0:T(8,128)(2,1)} async-done(((bf16[8,4,48,2048]{3,2,1,0:T(8,128)(2,1)}), bf16[8,4,48,2048]{3,2,1,0:T(8,128)(2,1)}) %all-reduce.3.cloned.1.call-update) | async-done | bytes 6291472
  281.3 3.4 constant_dynamic-slice_fusion
  284.7 5.6 %all-to-all-start.1 = ((bf16[8,1,48,2048]{3,2,1,0:T(8,128)(2,1)}), bf16[8,1,48,2048]{3,2,1,0:T(8,128)(2,1)}, u32[]{:S(2)}, u32[]{:S(2)}) async-start(bf16[8,1,48,2048]{3,2,1,0:T(8,128)(2,1)} %constant_dynamic-slice_fusion), calls=%async_computation.2 | async-start | bytes 3145728 | tf_op jit(solution)/shard_map/all_to_all | solution.py:106
  290.7 34.1 %all-to-all-done.1 = bf16[8,1,48,2048]{3,2,1,0:T(8,128)(2,1)} async-done(((bf16[8,1,48,2048]{3,2,1,0:T(8,128)(2,1)}), bf16[8,1,48,2048]{3,2,1,0:T(8,128)(2,1)}, u32[]{:S(2)}, u32[]{:S(2)}) %all-to-all-start.1) | async-done | bytes 1572896 | tf_op jit(solution)/shard_map/all_to_all | solution.py:106
  324.8 5.0 %gather_fusion.1 = bf16[256,2048]{1,0:T(8,128)(2,1)} fusion(bf16[384,2048]{1,0:T(8,128)(2,1)} %bitcast.12, s32[1024]{0:T(1024)S(1)} %pad_clamp_fusion), kind=kCustom, calls=%fused_computation.1 | custom fusion | bytes 2098176 | tf_op jit(solution)/shard_map/gather | solution.py:108
  329.7 3.4 reshape.205
  333.1 4.9 %multiply_reduce_fusion = f32[128,2048]{1,0:T(8,128)S(1)} fusion(f32[128,2,2048]{2,1,0:T(2,128)} %reshape.205, f32[128,2]{1,0:T(8,128)S(1)} %copy.24), kind=kLoop, calls=%fused_computation.6 | loop fusion | flops 786432 | bytes 3146752 | tf_op jit(solution)/shard_map/reduce_sum | solution.py:109
  338.0 1.0 fusion.5
  (47 shorter events, 1.7 us)
Async XLA Ops:
  6.5 10.2 %copy-start = (bf16[512,2048]{1,0:T(8,128)(2,1)S(1)}, bf16[512,2048]{1,0:T(8,128)(2,1)}, u32[]{:S(2)}) copy-start(bf16[512,2048]{1,0:T(8,128)(2,1)} %param.17) | copy-start | bytes 6291460
  6.5 49.3 %reduce-scatter.5.cloned.1.call-start = ((), (), s32[]{:S(2)}) async-start(), calls=%async_computation.3 | async-start | bytes 2621440 | tf_op jit(solution)/shard_map/reduce_scatter | solution.py:78
  7.5 7.0 %collective-permute-start.1 = (bf16[15]{0:T(256)(128)(2,1)S(1)}, bf16[15]{0:T(256)(128)(2,1)S(1)}, u32[]{:S(2)}, u32[]{:S(2)}) collective-permute-start(bf16[15]{0:T(256)(128)(2,1)S(1)} %slice.108), channel_id=1, source_target_pairs={{0,4},{4,8},{8,12},{12,16},{16,20},{20,24},{24,28},{1,5},{5,9},{9,... | collective-permute-start | bytes 98 | tf_op jit(solution)/shard_map/ppermute | solution.py:15
  11.3 4.4 %collective-permute-start = (bf16[15,256]{1,0:T(8,128)(2,1)S(1)}, bf16[15,256]{1,0:T(8,128)(2,1)S(1)}, u32[]{:S(2)}, u32[]{:S(2)}) collective-permute-start(bf16[15,256]{1,0:T(8,128)(2,1)S(1)} %slice.106), channel_id=1, source_target_pairs={{0,4},{4,8},{8,12},{12,16},{16,20},{20,24},{24,28},{1,5},{5,9},{9,... | collective-permute-start | bytes 23048 | tf_op jit(solution)/shard_map/ppermute | solution.py:15
  22.1 33.7 %copy-start.1 = (bf16[128,2048]{1,0:T(8,128)(2,1)S(1)}, bf16[128,2048]{1,0:T(8,128)(2,1)}, u32[]{:S(2)}) copy-start(bf16[128,2048]{1,0:T(8,128)(2,1)} %param.12) | copy-start | bytes 1572868
  22.1 35.0 %copy-start.4 = (f32[2048]{0:T(1024)S(1)}, f32[2048]{0:T(1024)}, u32[]{:S(2)}) copy-start(f32[2048]{0:T(1024)} %param.18) | copy-start | bytes 24580
  22.2 128.4 %all-gather.2.cloned.1.call-start = ((), (), s32[]{:S(2)}) async-start(), calls=%async_computation.4 | async-start | bytes 7864320 | tf_op jit(solution)/shard_map/all_gather | solution.py:95
  102.4 178.9 %all-reduce.3.cloned.1.call-start = ((), (), s32[]{:S(2)}) async-start(), calls=%async_computation.5 | async-start | bytes 12582912
  150.6 5.1 %copy-start.6 = (bf16[8,4,48,2048]{3,2,1,0:T(8,128)(2,1)S(1)}, bf16[8,4,48,2048]{3,2,1,0:T(8,128)(2,1)}, u32[]{:S(2)}) copy-start(bf16[8,4,48,2048]{3,2,1,0:T(8,128)(2,1)} %all-gather.2.cloned.1.call-done) | copy-start | bytes 18874372
  150.6 5.1 %copy-start.7 = (bf16[1,2048,256]{2,1,0:T(8,128)(2,1)S(1)}, bf16[1,2048,256]{2,1,0:T(8,128)(2,1)}, u32[]{:S(2)}) copy-start(bf16[1,2048,256]{2,1,0:T(8,128)(2,1)} %param.22) | copy-start | bytes 3145732
  155.8 2.1 copy-start.3
  162.3 0.7 copy-start.8
  284.7 5.9 %copy-start.5 = (f32[128,2]{0,1:T(2,128)S(1)}, f32[128,2]{0,1:T(2,128)}, u32[]{:S(2)}) copy-start(f32[128,2]{0,1:T(2,128)} %param.20) | copy-start | bytes 3076
  284.7 40.1 %all-to-all-start.1 = ((bf16[8,1,48,2048]{3,2,1,0:T(8,128)(2,1)}), bf16[8,1,48,2048]{3,2,1,0:T(8,128)(2,1)}, u32[]{:S(2)}, u32[]{:S(2)}) async-start(bf16[8,1,48,2048]{3,2,1,0:T(8,128)(2,1)} %constant_dynamic-slice_fusion), calls=%async_computation.2 | async-start | bytes 3145728 | tf_op jit(solution)/shard_map/all_to_all | solution.py:106
  333.1 4.9 %copy-start.2 = (bf16[128,2048]{1,0:T(8,128)(2,1)S(1)}, bf16[128,2048]{1,0:T(8,128)(2,1)}, u32[]{:S(2)}) copy-start(bf16[128,2048]{1,0:T(8,128)(2,1)} %reduce-scatter.5.cloned.1.call-done) | copy-start | bytes 1572868
Sparse Core Ops, SparseCore 0:
  22.3 33.4 reduce-scatter.4
  102.5 48.0 all-gather.1
  162.5 118.7 all-reduce.2
where the time goes:
time: 350 us; the launch traced here: 346 us
  waiting for transfers between devices  231 us (66%)
  blocking collectives  39.2 us (11%)
  local copies, waits for them, and re-layouts  18.2 us (5%)
  matrix products  17 us (5%)
  other arithmetic  14.5 us (4%)
  between operations  13.3 us (4%)
  starting transfers between devices  12 us (3%)
    unnamed x4, waiting for transfers between devices  118 us
    all_gather x1, waiting for transfers between devices, per_device(): arrived = lax.all_gather(arrived, 'tp', axis=1, tiled=True)  48.2 us
    all_to_all x1, blocking collectives, per_device(): lax.all_to_all(dispatch, 'sp', split_axis=0, concat_axis=0, tiled=True)  39.2 us
    all_to_all x1, waiting for transfers between devices, per_device(): lax.all_to_all(summed, 'sp', split_axis=0, concat_axis=0, tiled=True)  34.1 us
    reduce_scatter x1, waiting for transfers between devices, per_device(): lax.psum_scatter(jnp.dot(branch, out_weight, preferred_element_type=jnp.f...  30.9 us
  transfers between devices with their start and end apart: 6, of which 5 were waited for; matrix products, arithmetic and copies ran while one was open for 1% of the time, Pallas kernels for 0%

commit v1 on v0

v1 whole, which is shorter than its diff:
```python
import functools

import jax
import jax.numpy as jnp
from jax import lax
from jax.experimental import pallas as pl
from jax.experimental.pallas import tpu as pltpu
from jax.sharding import PartitionSpec as P

HALO = 16
EPS = 1e-06
MESH = pl.DeviceIdType.MESH
F32 = jnp.float32
BF16 = jnp.bfloat16


def kernel(
    n_sp, n_tp, quarter, capacity, top,
    stream, pool_in, docs, pool_map, pool_scale, out_weight, gain, routes, weights,
    gate, up, down,
    out,
    gates, ups, downs, outw, halo, halo_docs, branch, pair_send, pair_recv, far_send, far_recv,
    mixed, dispatch, arrived, acc, answers, returned,
    local_sem, halo_ssem, halo_rsem, w_ssem, w_rsem, f_ssem, p_ssem, p_rsem,
    y_ssem, y_rsem, d_ssem, d_rsem, r_ssem, r_rsem,
):
    sp, tp = lax.axis_index("sp"), lax.axis_index("tp")
    n_chip = n_tp // 2
    chip, parity = tp // 2, tp % 2
    other = 1 - parity
    partner = chip * 2 + other
    rows = pool_in.shape[0]
    width = stream.shape[1]
    ff = gate.shape[1]
    slots = n_sp * capacity

    def same(m):
        return (chip + m) % n_chip * 2 + parity

    def remote(src, dst, ssem, rsem, to):
        return pltpu.make_async_remote_copy(
            src_ref=src, dst_ref=dst, send_sem=ssem, recv_sem=rsem,
            device_id=to, device_id_type=MESH,
        )

    half = width // 2
    pieces = (
        (gate.at[pl.ds(0, half)], lambda j: gates.at[j, pl.ds(0, half)]),
        (gate.at[pl.ds(half, half)], lambda j: gates.at[j, pl.ds(half, half)]),
        (up, lambda j: ups.at[j]),
        (down, lambda j: downs.at[j]),
    )
    count = len(pieces)

    own_copies = [
        pltpu.make_async_copy(out_weight, outw, local_sem.at[0]),
        pltpu.make_async_copy(gate, gates.at[0], local_sem.at[1]),
        pltpu.make_async_copy(up, ups.at[0], local_sem.at[2]),
        pltpu.make_async_copy(down, downs.at[0], local_sem.at[3]),
    ]
    for c in own_copies:
        c.start()

    barrier = pltpu.get_barrier_semaphore()
    for d in range(1, n_sp):
        pl.semaphore_signal(barrier, inc=1, device_id=((sp + d) % n_sp, tp), device_id_type=MESH)
    pl.semaphore_signal(barrier, inc=1, device_id=(sp, partner), device_id_type=MESH)
    for m in range(1, n_chip):
        pl.semaphore_signal(barrier, inc=1, device_id=(sp, same(m)), device_id_type=MESH)
    pl.semaphore_wait(barrier, n_sp - 1 + 1 + n_chip - 1)

    right = ((sp + 1) % n_sp, tp)
    halo_copies = [
        remote(pool_in.at[pl.ds(rows - HALO, HALO)], halo, halo_ssem.at[0], halo_rsem.at[0], right),
        remote(docs.at[pl.ds(rows - HALO, HALO)], halo_docs, halo_ssem.at[1], halo_rsem.at[1], right),
    ]
    for c in halo_copies:
        c.start()

    def far_weight(p, m):
        j = 2 * ((n_chip - m) % n_chip)
        return remote(pieces[p][0], pieces[p][1](j), w_ssem.at[m, p], w_rsem.at[j, p], (sp, same(m)))

    def near_weight(p):
        return remote(pieces[p][0], pieces[p][1](1), w_ssem.at[0, p], w_rsem.at[1, p], (sp, partner))

    def forward(p, m):
        ref = pieces[p][1](2 * m)
        return remote(ref, pieces[p][1](2 * m + 1), f_ssem.at[m, p], w_rsem.at[2 * m + 1, p], (sp, partner))

    for m in range(1, n_chip):
        far_weight(0, m).start()

    lanes = lax.broadcasted_iota(jnp.int32, (quarter, 128), 1)
    own_routes = routes[pl.ds(pl.multiple_of(tp * quarter, quarter), quarter), :]
    hots = [(own_routes[:, k : k + 1] == lanes).astype(F32) for k in range(top)]
    named = functools.reduce(lambda a, b: a + b, hots)
    below = (
        lax.broadcasted_iota(jnp.int32, (quarter, quarter), 0)
        > lax.broadcasted_iota(jnp.int32, (quarter, quarter), 1)
    ).astype(BF16)
    before = jnp.dot(below, named.astype(BF16), preferred_element_type=F32)
    slot_lanes = lax.broadcasted_iota(jnp.int32, (quarter, slots), 1)
    picks = []
    for k in range(top):
        rank = jnp.sum(hots[k] * before, axis=1, keepdims=True).astype(jnp.int32)
        picks.append((slot_lanes == own_routes[:, k : k + 1] * capacity + rank).astype(F32))
    spread = jnp.transpose(functools.reduce(lambda a, b: a + b, picks)).astype(BF16)
    picks = [p.astype(BF16) for p in picks]

    for c in halo_copies:
        c.wait_recv()
    first = sp == 0
    prior = jnp.where(first, 0.0, halo[...].astype(F32))
    prior_docs = jnp.where(first, -1, halo_docs[...])
    own = pool_in[...].astype(F32)
    group_width = own.shape[1]
    ext_docs = jnp.concatenate([prior_docs, docs[...]], axis=0)
    total = jnp.concatenate([prior, own], axis=0)
    counts = jnp.ones(ext_docs.shape, F32)
    window = jnp.left_shift(jnp.int32(2), tp)
    step = 1
    while step < HALO:
        keep = (pltpu.roll(ext_docs, step, 0) == ext_docs) & (step < window)
        counts = counts + jnp.where(keep, pltpu.roll(counts, step, 0), 0.0)
        keep_wide = jnp.concatenate([keep.astype(F32)] * (group_width // 128), axis=1) > 0.5
        total = total + jnp.where(keep_wide, pltpu.roll(total, step, 0), 0.0)
        step *= 2
    counts_wide = jnp.concatenate([counts] * (group_width // 128), axis=1)
    pooled = (total[HALO:] / counts_wide[HALO:] - own).astype(BF16)
    branch[...] = (
        jnp.dot(pooled, pool_map[...], preferred_element_type=F32) * pool_scale[...]
    ).astype(BF16)

    own_copies[0].wait()

    def share(owner):
        begin = pl.multiple_of(owner * quarter, quarter)
        return jnp.dot(branch[pl.ds(begin, quarter), :], outw[...], preferred_element_type=F32)

    pair_copies = []
    chips = list(range(1, n_chip)) + [0]
    for m in chips:
        pair_send[m] = share((chip + m) % n_chip * 2 + other).astype(BF16)
        c = remote(pair_send.at[m], pair_recv.at[m], p_ssem.at[m], p_rsem.at[m], (sp, partner))
        c.start()
        pair_copies.append(c)
    far_copies = []
    mine = None
    for m, c in zip(chips, pair_copies):
        block = share(same(m))
        c.wait_recv()
        block = block + pair_recv[m].astype(F32)
        if m == 0:
            mine = block
        else:
            far_send[m] = block.astype(BF16)
            j = (n_chip - m) % n_chip
            f = remote(far_send.at[m], far_recv.at[j], y_ssem.at[m], y_rsem.at[j], (sp, same(m)))
            f.start()
            far_copies.append(f)
            for p in range(1, count):
                far_weight(p, m).start()
    for p in range(count):
        near_weight(p).start()
    for m, f in zip(chips, far_copies):
        f.wait_recv()
        mine = mine + far_recv[(n_chip - m) % n_chip].astype(F32)
    mixed[...] = (stream[...].astype(F32) + mine).astype(BF16)
    value = mixed[...].astype(F32)
    normed = (
        value * lax.rsqrt(jnp.mean(value * value, axis=1, keepdims=True) + EPS) * gain[...]
    ).astype(BF16)

    dispatch[...] = jnp.dot(spread, normed, preferred_element_type=F32).astype(BF16)

    def part(ref, e):
        return ref.at[pl.ds(pl.multiple_of(e * capacity, 16), capacity)]

    def to_peer(src, dst, ssem, rsem, d):
        peer = (sp + d) % n_sp
        return remote(part(src, peer), part(dst, sp), ssem.at[d], rsem.at[d], (peer, tp))

    outward = [to_peer(dispatch, arrived, d_ssem, d_rsem, d) for d in range(1, n_sp)]
    for c in outward:
        c.start()
    mine_at = pl.ds(pl.multiple_of(sp * capacity, 16), capacity)
    arrived[mine_at, :] = dispatch[mine_at, :]

    for p in range(count - 1):
        for m in range(1, n_chip):
            remote(pieces[p][0], pieces[p][1](2 * m), w_ssem.at[m, p], w_rsem.at[2 * m, p], (sp, partner)).wait_recv()
            forward(p, m).start()
    for c in own_copies[1:]:
        c.wait()
    for c in outward:
        c.wait_recv()

    cols = 512

    def expert(j):
        x = arrived[...]
        g = jnp.dot(x, gates[j], preferred_element_type=F32)
        u = jnp.dot(x, ups[j], preferred_element_type=F32)
        return (g / (1.0 + jnp.exp(-g)) * u).astype(BF16)

    def project(j, hidden, begin):
        at = pl.ds(begin, cols)
        return jnp.dot(hidden, downs[j, :, at], preferred_element_type=F32).astype(BF16).astype(F32)

    for j in range(n_tp):
        if j % 2 == 1:
            for p in range(count - 1):
                remote(pieces[p][0], pieces[p][1](j), w_ssem.at[0, p], w_rsem.at[j, p], (sp, partner)).wait_recv()
        hidden = expert(j)
        p = count - 1
        if j >= 2 and j % 2 == 0:
            m = j // 2
            remote(pieces[p][0], pieces[p][1](j), w_ssem.at[m, p], w_rsem.at[j, p], (sp, partner)).wait_recv()
            forward(p, m).start()
        if j % 2 == 1:
            remote(pieces[p][0], pieces[p][1](j), w_ssem.at[0, p], w_rsem.at[j, p], (sp, partner)).wait_recv()
        for begin in range(0, width, cols):
            at = pl.ds(begin, cols)
            y = project(j, hidden, begin)
            if j == 0:
                acc[:, at] = y
            elif j < n_tp - 1:
                acc[:, at] += y
            else:
                answers[:, at] = (acc[:, at] + y).astype(BF16)

    back = [to_peer(answers, returned, r_ssem, r_rsem, d) for d in range(1, n_sp)]
    for c in back:
        c.start()
    returned[mine_at, :] = answers[mine_at, :]
    for c in back:
        c.wait_recv()
    for begin in range(0, width, cols):
        at = pl.ds(begin, cols)
        result = mixed[:, at].astype(F32)
        for k in range(top):
            result = result + weights[:, k : k + 1] * jnp.dot(
                picks[k], returned[:, at], preferred_element_type=F32
            )
        out[:, at] = result.astype(BF16)

    for c in halo_copies + pair_copies + far_copies + outward + back:
        c.wait_send()
    for p in range(count):
        near_weight(p).wait_send()
        for m in range(1, n_chip):
            far_weight(p, m).wait_send()
            forward(p, m).wait_send()


def per_device(
    n_sp, n_tp,
    stream, pool_in, doc_ids, pool_map, pool_scale, out_weight, norm_gain, routes, route_weight,
    expert_gate, expert_up, expert_down,
):
    rows, group_width = pool_in.shape
    quarter, width = stream.shape
    top = routes.shape[1]
    ff = expert_gate.shape[2]
    capacity = max(2, 3 * top * quarter // (2 * n_sp))
    capacity = -(-capacity // 16) * 16
    slots = n_sp * capacity
    n_chip = n_tp // 2
    vmem = pl.BlockSpec(memory_space=pltpu.VMEM)
    hbm = pl.BlockSpec(memory_space=pl.ANY)
    dma = pltpu.SemaphoreType.DMA
    V = pltpu.VMEM
    branch_width = out_weight.shape[0]
    return pl.pallas_call(
        functools.partial(kernel, n_sp, n_tp, quarter, capacity, top),
        out_shape=jax.ShapeDtypeStruct((quarter, width), BF16),
        in_specs=[vmem] * 5 + [hbm] + [vmem] * 3 + [hbm] * 3,
        out_specs=vmem,
        scratch_shapes=[
            V((n_tp, width, ff), BF16),
            V((n_tp, width, ff), BF16),
            V((n_tp, ff, width), BF16),
            V((branch_width, width), BF16),
            V((HALO, group_width), BF16),
            V((HALO, 128), jnp.int32),
            V((rows, branch_width), BF16),
            V((n_chip, quarter, width), BF16),
            V((n_chip, quarter, width), BF16),
            V((n_chip, quarter, width), BF16),
            V((n_chip, quarter, width), BF16),
            V((quarter, width), BF16),
            V((slots, width), BF16),
            V((slots, width), BF16),
            V((slots, width), F32),
            V((slots, width), BF16),
            V((slots, width), BF16),
            dma((4,)),
            dma((2,)),
            dma((2,)),
            dma((n_chip, 4)),
            dma((n_tp, 4)),
            dma((n_chip, 4)),
            dma((n_chip,)),
            dma((n_chip,)),
            dma((n_chip,)),
            dma((n_chip,)),
            dma((n_sp,)),
            dma((n_sp,)),
            dma((n_sp,)),
            dma((n_sp,)),
        ],
        compiler_params=pltpu.CompilerParams(
            collective_id=0, has_side_effects=True, vmem_limit_bytes=60 * 1024 * 1024
        ),
    )(
        stream, pool_in, jnp.broadcast_to(doc_ids[:, None], (rows, 128)), pool_map[0],
        pool_scale[None, :], out_weight, norm_gain[None, :], routes, route_weight,
        expert_gate[0], expert_up[0], expert_down[0],
    )


def solution(mesh):
    in_specs = (
        P(("sp", "tp"), None),
        P("sp", "tp"),
        P("sp"),
        P("tp", None, None),
        P("tp"),
        P("tp", None),
        P(),
        P("sp", None),
        P(("sp", "tp"), None),
        P("sp", None, "tp"),
        P("sp", None, "tp"),
        P("sp", "tp", None),
    )
    out_specs = P(("sp", "tp"), None)
    return jax.shard_map(
        functools.partial(per_device, mesh.shape["sp"], mesh.shape["tp"]),
        mesh=mesh, in_specs=in_specs, out_specs=out_specs, check_vma=False,
    )
```

time: 350 us -> 133 us (0.38); the launches traced: 346 us -> 133 us
  waiting for transfers between devices: 231 us -> 0 us
  Pallas kernels: 0 us -> 126 us
  blocking collectives: 39.2 us -> 0 us
  matrix products: 17 us -> 0 us
  other arithmetic: 14.5 us -> 0 us
  between operations: 13.3 us -> 0.01 us
  starting transfers between devices: 12 us -> 0 us
  local copies, waits for them, and re-layouts: 18.2 us -> 6.33 us
    pallas_call x0 -> x1, Pallas kernels: none -> 126 us  [per_device(): pl.pallas_call(functools.partial(kernel, n_sp, n_tp, quarter, capacity, t...]
    unnamed x4 -> x0, waiting for transfers between devices: 118 us -> none
    all_gather x1 -> x0, waiting for transfers between devices: 48.2 us -> none  [per_device(): arrived = lax.all_gather(arrived, 'tp', axis=1, tiled=True)]
    all_to_all x1 -> x0, blocking collectives: 39.2 us -> none  [per_device(): lax.all_to_all(dispatch, 'sp', split_axis=0, concat_axis=0, tiled=True)]
    all_to_all x1 -> x0, waiting for transfers between devices: 34.1 us -> none  [per_device(): lax.all_to_all(summed, 'sp', split_axis=0, concat_axis=0, tiled=True)]
    reduce_scatter x1 -> x0, waiting for transfers between devices: 30.9 us -> none  [per_device(): lax.psum_scatter(jnp.dot(branch, out_weight, preferred_element_type=jnp.f...]
    dot_general x4 -> x0, matrix products: 17 us -> none  [the longest x1 5.4 us: per_device(): jnp.dot(branch, out_weight, preferred_element_type=jnp.float32)]
    gather x2 -> x0, local copies, waits for them, and re-layouts: 8.09 us -> none  [the longest x1 4.96 us: per_device(): outputs[own_slots].astype(jnp.float32)]
  transfers between devices with their start and end apart: 6 -> 0, of which waited for: 5 -> 0; matrix products, arithmetic and copies ran while one was open for 1% -> 0% of each run, Pallas kernels for 0% -> 0%
where the time goes in v1:
time: 133 us
  Pallas kernels  126 us (95%)
  local copies, waits for them, and re-layouts  6.33 us (5%)
    pallas_call x1, Pallas kernels, per_device(): pl.pallas_call(functools.partial(kernel, n_sp, n_tp, quarter, capacity, t...  126 us
    unnamed x3, local copies, waits for them, and re-layouts  4.82 us

profile of v1, /device:TPU:11, one launch (start us, length us, event | category | flops | bytes accessed | tf_op | source)
XLA Modules:
  0.0 132.6 jit_solution(8629511224744171039)
XLA Ops:
  0.0 1.4 %copy.14.weights = f32[128,2]{1,0:T(8,128)} copy(f32[128,2]{0,1:T(2,128)} %param.20) | data formatting | bytes 2048 | tf_op args[8]
  1.4 1.5 %broadcast_in_dim.12.docs = s32[512,128]{1,0:T(8,128)} broadcast(s32[512]{0:T(512)} %param.14), dimensions={0} | broadcast | bytes 264192 | tf_op jit(solution)/shard_map/broadcast_in_dim | solution.py:317
  2.9 1.5 %copy.13.routes = s32[512,2]{1,0:T(8,128)} copy(s32[512,2]{0,1:T(2,128)} %param.19) | data formatting | bytes 8192 | tf_op args[7]
  4.5 126.2 %shard_map.118 = bf16[128,2048]{1,0:T(8,128)(2,1)} custom-call(bf16[128,2048]{1,0:T(8,128)(2,1)} %stream.1, bf16[512,256]{1,0:T(8,128)(2,1)} %pool_in.1, s32[512,128]{1,0:T(8,128)} %broadcast_in_dim.12.docs, bf16[256,512]{1,0:T(8,128)(2,1)} %bitcast.9, f32[1,512]{1,0:T(1,128)} %bitcast.11, bf16[512,2048]{1,0:T(8,128)(2,1)} %out_weight.1, ...), custom_call_target="tpu_custom_call" | custom-call | tf_op jit(solution)/shard_map/pallas_call | solution.py:275
  130.7 1.9 %copy.16 = bf16[128,2048]{1,0:T(8,128)(2,1)} copy(bf16[128,2048]{1,0:T(8,128)(2,1)} %shard_map.118) | data formatting | bytes 1048576

commit v2 on v1

--- a/solution.py
+++ b/solution.py
@@ -8,6 +8,7 @@
 from jax.sharding import PartitionSpec as P
 
 HALO = 16
+COLS = 512
 EPS = 1e-06
 MESH = pl.DeviceIdType.MESH
 F32 = jnp.float32
@@ -16,11 +17,11 @@
 
 def kernel(
     n_sp, n_tp, quarter, capacity, top,
-    stream, pool_in, docs, pool_map, pool_scale, out_weight, gain, routes, weights,
+    stream, pool_in, docs_row, pool_map, pool_scale, out_weight, gain, routes, weights,
     gate, up, down,
     out,
     gates, ups, downs, outw, halo, halo_docs, branch, pair_send, pair_recv, far_send, far_recv,
-    mixed, dispatch, arrived, acc, answers, returned,
+    mixed, dispatch, arrived, hiddens, answers, returned, docs,
     local_sem, halo_ssem, halo_rsem, w_ssem, w_rsem, f_ssem, p_ssem, p_rsem,
     y_ssem, y_rsem, d_ssem, d_rsem, r_ssem, r_rsem,
 ):
@@ -48,9 +49,15 @@
         (gate.at[pl.ds(0, half)], lambda j: gates.at[j, pl.ds(0, half)]),
         (gate.at[pl.ds(half, half)], lambda j: gates.at[j, pl.ds(half, half)]),
         (up, lambda j: ups.at[j]),
-        (down, lambda j: downs.at[j]),
+    ) + tuple(
+        (
+            down.at[:, pl.ds(begin, COLS)],
+            lambda j, begin=begin: downs.at[j, :, pl.ds(begin, COLS)],
+        )
+        for begin in range(0, width, COLS)
     )
     count = len(pieces)
+    early = 3
 
     own_copies = [
         pltpu.make_async_copy(out_weight, outw, local_sem.at[0]),
@@ -69,6 +76,7 @@
         pl.semaphore_signal(barrier, inc=1, device_id=(sp, same(m)), device_id_type=MESH)
     pl.semaphore_wait(barrier, n_sp - 1 + 1 + n_chip - 1)
 
+    docs[...] = jnp.transpose(jnp.broadcast_to(docs_row[...].astype(F32), (128, rows)))
     right = ((sp + 1) % n_sp, tp)
     halo_copies = [
         remote(pool_in.at[pl.ds(rows - HALO, HALO)], halo, halo_ssem.at[0], halo_rsem.at[0], right),
@@ -91,28 +99,32 @@
     for m in range(1, n_chip):
         far_weight(0, m).start()
 
-    lanes = lax.broadcasted_iota(jnp.int32, (quarter, 128), 1)
-    own_routes = routes[pl.ds(pl.multiple_of(tp * quarter, quarter), quarter), :]
-    hots = [(own_routes[:, k : k + 1] == lanes).astype(F32) for k in range(top)]
+    names = lax.broadcasted_iota(jnp.int32, (128, quarter), 0)
+    own_routes = routes[:, pl.ds(pl.multiple_of(tp * quarter, quarter), quarter)]
+    hots = [(own_routes[k : k + 1, :] == names).astype(F32) for k in range(top)]
     named = functools.reduce(lambda a, b: a + b, hots)
-    below = (
+    above = (
         lax.broadcasted_iota(jnp.int32, (quarter, quarter), 0)
-        > lax.broadcasted_iota(jnp.int32, (quarter, quarter), 1)
+        < lax.broadcasted_iota(jnp.int32, (quarter, quarter), 1)
     ).astype(BF16)
-    before = jnp.dot(below, named.astype(BF16), preferred_element_type=F32)
-    slot_lanes = lax.broadcasted_iota(jnp.int32, (quarter, slots), 1)
-    picks = []
+    before = jnp.dot(named.astype(BF16), above, preferred_element_type=F32)
+    slot_names = lax.broadcasted_iota(jnp.int32, (slots, quarter), 0)
+    places = []
     for k in range(top):
-        rank = jnp.sum(hots[k] * before, axis=1, keepdims=True).astype(jnp.int32)
-        picks.append((slot_lanes == own_routes[:, k : k + 1] * capacity + rank).astype(F32))
-    spread = jnp.transpose(functools.reduce(lambda a, b: a + b, picks)).astype(BF16)
-    picks = [p.astype(BF16) for p in picks]
+        rank = jnp.sum(hots[k] * before, axis=0, keepdims=True).astype(jnp.int32)
+        places.append((slot_names == own_routes[k : k + 1, :] * capacity + rank).astype(F32))
+    spread = functools.reduce(lambda a, b: a + b, places).astype(BF16)
+    picks = [jnp.transpose(p).astype(BF16) for p in places]
+    scales = [
+        jnp.transpose(jnp.broadcast_to(weights[k : k + 1, :], (128, quarter)))[:, :1]
+        for k in range(top)
+    ]
 
     for c in halo_copies:
         c.wait_recv()
     first = sp == 0
     prior = jnp.where(first, 0.0, halo[...].astype(F32))
-    prior_docs = jnp.where(first, -1, halo_docs[...])
+    prior_docs = jnp.where(first, -1.0, halo_docs[...])
     own = pool_in[...].astype(F32)
     group_width = own.shape[1]
     ext_docs = jnp.concatenate([prior_docs, docs[...]], axis=0)
@@ -174,73 +186,73 @@
 
     dispatch[...] = jnp.dot(spread, normed, preferred_element_type=F32).astype(BF16)
 
-    def part(ref, e):
-        return ref.at[pl.ds(pl.multiple_of(e * capacity, 16), capacity)]
-
-    def to_peer(src, dst, ssem, rsem, d):
+    def part(ref, e, at):
+        return ref.at[pl.ds(pl.multiple_of(e * capacity, 16), capacity), at]
+
+    def to_peer(src, dst, ssem, rsem, d, at):
         peer = (sp + d) % n_sp
-        return remote(part(src, peer), part(dst, sp), ssem.at[d], rsem.at[d], (peer, tp))
-
-    outward = [to_peer(dispatch, arrived, d_ssem, d_rsem, d) for d in range(1, n_sp)]
+        return remote(part(src, peer, at), part(dst, sp, at), ssem, rsem, (peer, tp))
+
+    everything = pl.ds(0, width)
+    outward = [
+        to_peer(dispatch, arrived, d_ssem.at[d], d_rsem.at[d], d, everything)
+        for d in range(1, n_sp)
+    ]
     for c in outward:
         c.start()
     mine_at = pl.ds(pl.multiple_of(sp * capacity, 16), capacity)
     arrived[mine_at, :] = dispatch[mine_at, :]
 
-    for p in range(count - 1):
+    def landed(p, j):
+        remote(
+            pieces[p][0], pieces[p][1](j), w_ssem.at[0, p], w_rsem.at[j, p], (sp, partner)
+        ).wait_recv()
+
+    for p in range(early):
         for m in range(1, n_chip):
-            remote(pieces[p][0], pieces[p][1](2 * m), w_ssem.at[m, p], w_rsem.at[2 * m, p], (sp, partner)).wait_recv()
+            landed(p, 2 * m)
             forward(p, m).start()
     for c in own_copies[1:]:
         c.wait()
     for c in outward:
         c.wait_recv()
 
-    cols = 512
-
-    def expert(j):
+    for j in range(n_tp):
+        if j % 2 == 1:
+            for p in range(early):
+                landed(p, j)
         x = arrived[...]
         g = jnp.dot(x, gates[j], preferred_element_type=F32)
         u = jnp.dot(x, ups[j], preferred_element_type=F32)
-        return (g / (1.0 + jnp.exp(-g)) * u).astype(BF16)
-
-    def project(j, hidden, begin):
-        at = pl.ds(begin, cols)
-        return jnp.dot(hidden, downs[j, :, at], preferred_element_type=F32).astype(BF16).astype(F32)
-
-    for j in range(n_tp):
-        if j % 2 == 1:
-            for p in range(count - 1):
-                remote(pieces[p][0], pieces[p][1](j), w_ssem.at[0, p], w_rsem.at[j, p], (sp, partner)).wait_recv()
-        hidden = expert(j)
-        p = count - 1
-        if j >= 2 and j % 2 == 0:
-            m = j // 2
-            remote(pieces[p][0], pieces[p][1](j), w_ssem.at[m, p], w_rsem.at[j, p], (sp, partner)).wait_recv()
+        hiddens[j] = (g / (1.0 + jnp.exp(-g)) * u).astype(BF16)
+
+    back = []
+    for p in range(early, count):
+        at = pl.ds((p - early) * COLS, COLS)
+        for m in range(1, n_chip):
+            landed(p, 2 * m)
             forward(p, m).start()
-        if j % 2 == 1:
-            remote(pieces[p][0], pieces[p][1](j), w_ssem.at[0, p], w_rsem.at[j, p], (sp, partner)).wait_recv()
-        for begin in range(0, width, cols):
-            at = pl.ds(begin, cols)
-            y = project(j, hidden, begin)
-            if j == 0:
-                acc[:, at] = y
-            elif j < n_tp - 1:
-                acc[:, at] += y
-            else:
-                answers[:, at] = (acc[:, at] + y).astype(BF16)
-
-    back = [to_peer(answers, returned, r_ssem, r_rsem, d) for d in range(1, n_sp)]
-    for c in back:
-        c.start()
-    returned[mine_at, :] = answers[mine_at, :]
-    for c in back:
-        c.wait_recv()
-    for begin in range(0, width, cols):
-        at = pl.ds(begin, cols)
+        total = None
+        for j in range(n_tp):
+            if j % 2 == 1:
+                landed(p, j)
+            y = jnp.dot(hiddens[j], downs[j, :, at], preferred_element_type=F32)
+            y = y.astype(BF16).astype(F32)
+            total = y if total is None else total + y
+        answers[:, at] = total.astype(BF16)
+        for d in range(1, n_sp):
+            c = to_peer(answers, returned, r_ssem.at[p - early, d], r_rsem.at[p - early, d], d, at)
+            c.start()
+            back.append(c)
+        returned[mine_at, at] = answers[mine_at, at]
+
+    for p in range(early, count):
+        at = pl.ds((p - early) * COLS, COLS)
+        for c in back[(p - early) * (n_sp - 1) : (p - early + 1) * (n_sp - 1)]:
+            c.wait_recv()
         result = mixed[:, at].astype(F32)
         for k in range(top):
-            result = result + weights[:, k : k + 1] * jnp.dot(
+            result = result + scales[k] * jnp.dot(
                 picks[k], returned[:, at], preferred_element_type=F32
             )
         out[:, at] = result.astype(BF16)
@@ -272,6 +284,7 @@
     dma = pltpu.SemaphoreType.DMA
     V = pltpu.VMEM
     branch_width = out_weight.shape[0]
+    pieces = 3 + width // COLS
     return pl.pallas_call(
         functools.partial(kernel, n_sp, n_tp, quarter, capacity, top),
         out_shape=jax.ShapeDtypeStruct((quarter, width), BF16),
@@ -283,7 +296,7 @@
             V((n_tp, ff, width), BF16),
             V((branch_width, width), BF16),
             V((HALO, group_width), BF16),
-            V((HALO, 128), jnp.int32),
+            V((HALO, 128), F32),
             V((rows, branch_width), BF16),
             V((n_chip, quarter, width), BF16),
             V((n_chip, quarter, width), BF16),
@@ -292,30 +305,31 @@
             V((quarter, width), BF16),
             V((slots, width), BF16),
             V((slots, width), BF16),
-            V((slots, width), F32),
+            V((n_tp, slots, ff), BF16),
             V((slots, width), BF16),
             V((slots, width), BF16),
+            V((rows, 128), F32),
             dma((4,)),
             dma((2,)),
             dma((2,)),
-            dma((n_chip, 4)),
-            dma((n_tp, 4)),
-            dma((n_chip, 4)),
+            dma((n_chip, pieces)),
+            dma((n_tp, pieces)),
+            dma((n_chip, pieces)),
             dma((n_chip,)),
             dma((n_chip,)),
             dma((n_chip,)),
             dma((n_chip,)),
             dma((n_sp,)),
             dma((n_sp,)),
-            dma((n_sp,)),
-            dma((n_sp,)),
+            dma((width // COLS, n_sp)),
+            dma((width // COLS, n_sp)),
         ],
         compiler_params=pltpu.CompilerParams(
             collective_id=0, has_side_effects=True, vmem_limit_bytes=60 * 1024 * 1024
         ),
     )(
-        stream, pool_in, jnp.broadcast_to(doc_ids[:, None], (rows, 128)), pool_map[0],
-        pool_scale[None, :], out_weight, norm_gain[None, :], routes, route_weight,
+        stream, pool_in, doc_ids[None, :], pool_map[0],
+        pool_scale[None, :], out_weight, norm_gain[None, :], routes.T, route_weight.T,
         expert_gate[0], expert_up[0], expert_down[0],
     )
 

time: 133 us -> 112 us (0.84)
  Pallas kernels: 126 us -> 110 us
  local copies, waits for them, and re-layouts: 6.33 us -> 1.88 us
    pallas_call x1, Pallas kernels: 126 us -> 110 us  [per_device(): pl.pallas_call(functools.partial(kernel, n_sp, n_tp, quarter, capacity, t...]
    unnamed x3 -> x1, local copies, waits for them, and re-layouts: 4.82 us -> 1.88 us
    broadcast_in_dim x1 -> x0, local copies, waits for them, and re-layouts: 1.52 us -> none  [per_device(): jnp.broadcast_to(doc_ids[:, None], (rows, 128))]
where the time goes in v2:
time: 112 us
  Pallas kernels  110 us (98%)
  local copies, waits for them, and re-layouts  1.88 us (2%)
    pallas_call x1, Pallas kernels, per_device(): pl.pallas_call(functools.partial(kernel, n_sp, n_tp, quarter, capacity, t...  110 us

profile of v2, /device:TPU:11, one launch (start us, length us, event | category | flops | bytes accessed | tf_op | source)
XLA Modules:
  0.0 111.5 jit_solution(12723170219597919790)
XLA Ops:
  0.0 109.6 %shard_map.118 = bf16[128,2048]{1,0:T(8,128)(2,1)} custom-call(bf16[128,2048]{1,0:T(8,128)(2,1)} %stream.1, bf16[512,256]{1,0:T(8,128)(2,1)} %pool_in.1, s32[1,512]{1,0:T(1,128)} %bitcast.15, bf16[256,512]{1,0:T(8,128)(2,1)} %bitcast.12, f32[1,512]{1,0:T(1,128)} %bitcast.16, bf16[512,2048]{1,0:T(8,128)(2,1)} %out_weight.1, f32[1,2048]{1,0:T(1,128)} %bitcast.13, ...), custom_call_target="tpu_custom_call" | custom-call | tf_op jit(solution)/shard_map/pallas_call | solution.py:288
  109.6 1.9 %copy.14 = bf16[128,2048]{1,0:T(8,128)(2,1)} copy(bf16[128,2048]{1,0:T(8,128)(2,1)} %shard_map.118) | data formatting | bytes 1048576
